TPU v7x, 512 devices: a whole 4x8x8 slice. The times are simulated.
512 devices in a mesh: sp: 32 (over z, x), tp: 16 (over y, core).
Axes of the slice: x: 4, y: 8, z: 8, core: 2. Of those that a mesh axis runs over, the one named last changes fastest.
Arguments:
- queries: bfloat16 [8192, 2048], P('sp', 'tp'), may hold values from -6 to 6
- key_matrix: bfloat16 [8192, 2048], P('sp', 'tp'), may hold values from -6 to 6
- value_matrix: bfloat16 [8192, 4096], P('sp', 'tp'), may hold values from -6 to 6
- output_gate_preactivation: bfloat16 [8192, 4096], P('sp', 'tp'), may hold values from -6 to 6
- decay_preactivation: bfloat16 [8192, 2048], P('sp', 'tp')
- extra_log_decay: float32 [8192, 16], P('sp', 'tp'), may hold values from -0.7 to 0
- head_norm_gain: bfloat16 [256], replicated, may hold values from 0.099609375 to 1.8984375
- output_projection: bfloat16 [4096, 2048], P(None, 'tp'), may hold values from -0.09375 to 0.09375
- residual: bfloat16 [8192, 2048], P('sp', 'tp'), may hold values from -210 to 210
- feedforward_gain: bfloat16 [2048], replicated, may hold values from 0.099609375 to 1.8984375
- routing: int32 [8192, 4], P('sp'), may hold values from 0 to 127, all different within a row; in each aligned block of 256 rows (0 to 255, 256 to 511, ...) at most 12 rows name the same one
- router_score: float32 [8192, 4], P('sp'), may hold values from 0.05 to 1
- expert_gate_weight: bfloat16 [2048, 131072], P(None, ('sp', 'tp')), may hold values from -0.125 to 0.125
- expert_up_weight: bfloat16 [2048, 131072], P(None, ('sp', 'tp')), may hold values from -0.125 to 0.125
- expert_down_weight: bfloat16 [131072, 2048], P(('sp', 'tp')), may hold values from -0.1875 to 0.1875
- shared_expert_gate: bfloat16 [2048, 512], P(None, 'tp'), may hold values from -0.125 to 0.125
- shared_expert_up: bfloat16 [2048, 512], P(None, 'tp'), may hold values from -0.125 to 0.125
- shared_expert_down: bfloat16 [512, 2048], P(None, 'tp'), may hold values from -0.25 to 0.25
Outputs:
- layer_out: bfloat16 [8192, 2048], P('sp', 'tp')
Inputs may be any that keep to these rules, and one draw needn't show every extreme that they name: `routing`: each row names 4 different experts. In each aligned block of 256 rows, the rows of one index of sp, no expert is named by more than 12 rows, a bound that some expert reaches in some blocks.
All inputs are finite; a program needn't handle non-finite values.
Results may differ from a plain program's by a relative error of at most 0.01.
Values may be sent and summed in bfloat16 or wider, within the bound.
No kernel may reach another device: no remote copies, remote signals or barrier semaphores. Data moves between devices by JAX's collectives and lax.ppermute only.
A program may use at most 64 MiB of HBM per device.

v0:
```python
import jax
import jax.numpy as jnp
from jax import lax
from jax.sharding import Mesh
from jax.sharding import PartitionSpec as P

DK = 128
DV = 256
BLOCK_POSITIONS = 64
FF_PARTS = 4
SP = ("sp_0", "sp_1")
SP_TP = ("sp_0", "sp_1", "tp")
HIGHEST = lax.Precision.HIGHEST
EPSILON = 1e-06
ROUTE_SCALE = 2.5
GATE_TEMPER = 16.0


def nothing_yet(value, identity):
    return jax.tree.map(
        lambda part, zero: jnp.zeros_like(part) + jnp.asarray(zero, part.dtype), value, identity
    )


def prefix_by_axis(value, axes, combine, identity):
    before = start = nothing_yet(value, identity)
    total = value
    for axis in reversed(axes):
        count, position = (lax.axis_size(axis), lax.axis_index(axis))
        pieces = jax.tree.map(
            lambda part, kind: lax.all_gather(part.astype(kind), axis),
            total,
            (jnp.bfloat16, jnp.bfloat16),
        )
        inside, total = (start, start)
        for k in range(count):
            passed = k < position
            total = combine(
                total, jax.tree.map(lambda part, own: part[k].astype(own.dtype), pieces, value)
            )
            inside = jax.tree.map(lambda new, old: jnp.where(passed, new, old), total, inside)
        before = combine(inside, before)
    return before


def laid_out(blocks, dim):
    blocks = jnp.moveaxis(blocks, 0, dim)
    dims = blocks.shape
    return blocks.reshape(*dims[:dim], dims[dim] * dims[dim + 1], *dims[dim + 2 :])


def sent_to_all(value, axis):
    copies = jnp.broadcast_to(value, (lax.axis_size(axis), *value.shape))
    return lax.all_to_all(copies, axis, split_axis=0, concat_axis=0, tiled=True)


def gather_directly(value, axis, dim):
    return laid_out(sent_to_all(value, axis), dim)


def from_partner(value, axis, bit):
    mask = 2**bit
    pairs = [(source, source ^ mask) for source in range(lax.axis_size(axis))]
    return lax.ppermute(value, axis, pairs)


def carry_combine(first_part, second_part):
    return (
        first_part[0] * second_part[0],
        second_part[0][..., None] * first_part[1] + second_part[1],
    )


def attention_heads(queries, key_matrix, value_matrix, decay_preactivation, extra_log_decay):
    tokens = queries.shape[0]
    local_head_count = extra_log_decay.shape[1]
    block_count = tokens // BLOCK_POSITIONS
    query_block = queries.astype(jnp.float32).reshape(
        block_count, BLOCK_POSITIONS, local_head_count, DK
    ) * DK ** (-0.5)
    key_block = key_matrix.astype(jnp.float32).reshape(
        block_count, BLOCK_POSITIONS, local_head_count, DK
    )
    value_block = value_matrix.astype(jnp.float32).reshape(
        block_count, BLOCK_POSITIONS, local_head_count, DV
    )
    log_decay_rows = (
        jax.nn.log_sigmoid(decay_preactivation.astype(jnp.float32)).reshape(
            block_count, BLOCK_POSITIONS, local_head_count, DK
        )
        / GATE_TEMPER
    )
    log_decay_rows = (
        log_decay_rows
        + extra_log_decay.reshape(block_count, BLOCK_POSITIONS, local_head_count)[..., None]
    )
    inside = jnp.cumsum(log_decay_rows, axis=1)
    block_total = inside[:, -1]
    query_decay = query_block * jnp.exp(inside)
    key_decay = key_block * jnp.exp(-inside)
    causal = jnp.tril(jnp.ones((BLOCK_POSITIONS, BLOCK_POSITIONS), dtype=bool))
    scores = jnp.where(
        causal, jnp.einsum("nthd,nshd->nhts", query_decay, key_decay, precision=HIGHEST), 0.0
    )
    within = jnp.einsum("nhts,nshv->nthv", scores, value_block, precision=HIGHEST)
    key_end = key_block * jnp.exp(block_total[:, None] - inside)
    update = jnp.einsum("nshd,nshv->nhdv", key_end, value_block, precision=HIGHEST)
    before = jnp.cumsum(block_total, axis=0) - block_total
    ending = jnp.concatenate([before, (before[-1] + block_total[-1])[None]], axis=0)
    after_block = before + block_total
    earlier_mask = jnp.arange(block_count + 1)[:, None] > jnp.arange(block_count)[None, :]
    span_logs = jnp.where(
        earlier_mask[:, :, None, None], ending[:, None] - after_block[None], -1e30
    )
    states = jnp.einsum("nmhd,mhdv->nhdv", jnp.exp(span_logs), update, precision=HIGHEST)
    passed = jnp.einsum("nthd,nhdv->nthv", query_decay, states[:block_count], precision=HIGHEST)
    query_start = query_block * jnp.exp(inside + before[:, None])
    return (within + passed, query_start, jnp.exp(ending[block_count]), states[block_count])


def body(
    queries,
    key_matrix,
    value_matrix,
    output_gate_preactivation,
    decay_preactivation,
    extra_log_decay,
    head_norm_gain,
    output_projection,
    residual,
    feedforward_gain,
    routing,
    router_score,
    expert_gate_weight,
    expert_up_weight,
    expert_down_weight,
    shared_expert_gate,
    shared_expert_up,
    shared_expert_down,
):
    tokens = queries.shape[0]
    local_head_count = extra_log_decay.shape[1]
    local_part, query_start, dev_decay, dev_update = attention_heads(
        queries, key_matrix, value_matrix, decay_preactivation, extra_log_decay
    )
    _, entering = prefix_by_axis(
        (dev_decay, dev_update),
        SP,
        carry_combine,
        (jnp.ones_like(dev_decay), jnp.zeros_like(dev_update)),
    )
    attention_output = local_part + jnp.einsum(
        "nthd,hdv->nthv", query_start, entering, precision=HIGHEST
    )
    attention_output = attention_output.reshape(tokens, local_head_count, DV)
    inverse_rms = lax.rsqrt(
        jnp.mean(attention_output * attention_output, axis=-1, keepdims=True) + EPSILON
    )
    gate_act = jax.nn.silu(
        output_gate_preactivation.astype(jnp.float32).reshape(tokens, local_head_count, DV)
    )
    head_rows = (
        (attention_output * inverse_rms * head_norm_gain.astype(jnp.float32) * gate_act)
        .reshape(tokens, local_head_count * DV)
        .astype(jnp.bfloat16)
    )
    projected = jnp.dot(
        lax.all_gather(head_rows, "tp", axis=1, tiled=True),
        output_projection,
        preferred_element_type=jnp.float32,
    )
    mid_local = (residual.astype(jnp.float32) + projected).astype(jnp.bfloat16)
    mid_rows = gather_directly(mid_local, "tp", 1).astype(jnp.float32)
    normed = (
        mid_rows
        * lax.rsqrt(jnp.mean(mid_rows * mid_rows, axis=-1, keepdims=True) + EPSILON)
        * feedforward_gain.astype(jnp.float32)
    ).astype(jnp.bfloat16)
    shared_pre = jnp.dot(normed, shared_expert_gate, preferred_element_type=jnp.float32)
    shared_lin = jnp.dot(normed, shared_expert_up, preferred_element_type=jnp.float32)
    shared_hidden = (jax.nn.silu(shared_pre) * shared_lin).astype(jnp.bfloat16)
    senders = lax.axis_size(SP)
    tp_count = lax.axis_size("tp")
    tp_bits = tp_count.bit_length() - 1
    tp_index = lax.axis_index("tp")
    groups = tp_count // FF_PARTS
    group_here = tp_index // FF_PARTS
    part_here = tp_index % FF_PARTS
    model_width = normed.shape[1]
    picks = routing.shape[1]
    expert_total = senders * groups
    rows_most = max(2, 3 * tokens * picks // (2 * expert_total))
    slot_count = senders * rows_most
    flat_expert = routing.reshape(-1)
    one_hot = (flat_expert[:, None] == jnp.arange(expert_total, dtype=jnp.int32)[None, :]).astype(
        jnp.int32
    )
    rank_before = jnp.sum((jnp.cumsum(one_hot, axis=0) - one_hot) * one_hot, axis=1)
    owned = flat_expert % groups == group_here
    slot_index = jnp.where(owned, flat_expert // groups * rows_most + rank_before, slot_count)
    token_index = jnp.arange(flat_expert.shape[0], dtype=jnp.int32) // picks
    part_width = model_width // FF_PARTS
    normed_part = lax.dynamic_slice_in_dim(normed, part_here * part_width, part_width, 1)
    outgoing = (
        jnp.zeros((slot_count, part_width), jnp.bfloat16)
        .at[slot_index]
        .set(normed_part[token_index], mode="drop")
    )
    arrived = lax.all_to_all(
        outgoing.reshape(senders, rows_most, part_width),
        SP,
        split_axis=0,
        concat_axis=0,
        tiled=True,
    )
    for bit in range(2):
        partner_cols = from_partner(arrived, "tp", bit)
        upper = (tp_index >> bit) % 2
        arrived = jnp.where(
            upper == 1,
            jnp.concatenate([partner_cols, arrived], axis=2),
            jnp.concatenate([arrived, partner_cols], axis=2),
        )
    rows_in = arrived.reshape(slot_count, model_width)
    gate_pre = jnp.dot(rows_in, expert_gate_weight, preferred_element_type=jnp.float32)
    up_pre = jnp.dot(rows_in, expert_up_weight, preferred_element_type=jnp.float32)
    routed_hidden = (jax.nn.silu(gate_pre) * up_pre).astype(jnp.bfloat16)
    partial_out = jnp.dot(routed_hidden, expert_down_weight, preferred_element_type=jnp.float32)
    slab_width = model_width // tp_count
    partial_out = partial_out.reshape(slot_count, groups, FF_PARTS, slab_width)
    for bit in (1, 0):
        paired = partial_out.reshape(slot_count, groups, 2, 2**bit, slab_width)
        upper = (tp_index >> bit) % 2
        kept = lax.dynamic_index_in_dim(paired, upper, 2, keepdims=False)
        given = lax.dynamic_index_in_dim(paired, 1 - upper, 2, keepdims=False)
        partial_out = kept + from_partner(given.astype(jnp.bfloat16), "tp", bit).astype(given.dtype)
    expert_out = partial_out.reshape(senders, rows_most, groups, slab_width).astype(jnp.bfloat16)
    shared_out = jnp.dot(
        lax.all_gather(shared_hidden, "tp", axis=1, tiled=True),
        shared_expert_down,
        preferred_element_type=jnp.float32,
    )
    returned = lax.all_to_all(expert_out, SP, split_axis=0, concat_axis=0, tiled=True).reshape(
        slot_count, groups, slab_width
    )
    safe_slot = jnp.minimum(slot_index, slot_count - 1)
    route_weight = ROUTE_SCALE * router_score / jnp.sum(router_score, axis=1, keepdims=True)
    pair_weight = jnp.where(owned, route_weight.reshape(-1), 0.0)
    picked = returned[safe_slot].astype(jnp.float32) * pair_weight[:, None, None]
    routed_part = jnp.sum(picked.reshape(tokens, picks, groups, slab_width), axis=1)
    for bit in range(tp_bits - 1, 1, -1):
        paired = routed_part.reshape(tokens, 2, 2 ** (bit - 2), slab_width)
        upper = (tp_index >> bit) % 2
        kept = lax.dynamic_index_in_dim(paired, upper, 1, keepdims=False)
        given = lax.dynamic_index_in_dim(paired, 1 - upper, 1, keepdims=False)
        routed_part = kept + from_partner(given.astype(jnp.bfloat16), "tp", bit).astype(given.dtype)
    routed = routed_part.reshape(tokens, slab_width)
    return (mid_local.astype(jnp.float32) + routed + shared_out).astype(jnp.bfloat16)


def solution(mesh):
    finer = Mesh(mesh.devices.reshape(8, 4, mesh.shape["tp"]), ("sp_0", "sp_1", "tp"))
    in_specs = (
        P(SP, "tp"),
        P(SP, "tp"),
        P(SP, "tp"),
        P(SP, "tp"),
        P(SP, "tp"),
        P(SP, "tp"),
        P(),
        P(None, "tp"),
        P(SP, "tp"),
        P(),
        P(SP, None),
        P(SP, None),
        P(None, SP_TP),
        P(None, SP_TP),
        P(SP_TP, None),
        P(None, "tp"),
        P(None, "tp"),
        P(None, "tp"),
    )
    out_specs = P(SP, "tp")
    return jax.shard_map(body, mesh=finer, in_specs=in_specs, out_specs=out_specs, check_vma=False)
```

profile of v0, /device:TPU:1, one launch (start us, length us, event | category | flops | bytes accessed | tf_op | source)
XLA Modules:
  0.0 347.6 jit_solution(1330581877182747626)
XLA Ops:
  6.6 1.0 fusion.52
  7.6 0.5 broadcast.932
  8.1 1.3 reduce.7
  9.5 0.3 fusion.86
  10.2 1.4 fusion.49
  11.6 1.7 convolution_bitcast_fusion
  13.6 8.5 %all_gather.22 = bf16[4,1,128]{2,1,0:T(2,128)(2,1)S(1)} all-gather(bf16[1,1,128]{2,1,0:T(2,128)(2,1)S(1)} %get-tuple-element.7), channel_id=1, replica_groups=mesh['sp_0'=8,'sp_1'=4,'tp'=16] {'sp_1'}, dimensions={0}, use_global_device_ids=true | all-gather | bytes 1280 | tf_op jit(solution)/shard_map/all_gather | solution.py:31
  22.1 18.6 %all_gather.23 = bf16[8,1,128]{2,1,0:T(2,128)(2,1)S(1)} all-gather(bf16[1,1,128]{2,1,0:T(2,128)(2,1)S(1)} %multiply_convert_fusion.1), channel_id=1, replica_groups=mesh['sp_0'=8,'sp_1'=4,'tp'=16] {'sp_0'}, dimensions={0}, use_global_device_ids=true | all-gather | bytes 2304 | tf_op jit(solution)/shard_map/all_gather | solution.py:31
  40.7 0.6 fusion.124
  41.2 0.6 fusion.131
  41.9 0.4 convolution_select_fusion
  42.3 0.3 convolution_bitcast_fusion.2
  42.6 9.4 %all_gather.24 = bf16[4,1,128,256]{3,2,1,0:T(8,128)(2,1)S(1)} all-gather(bf16[1,1,128,256]{3,2,1,0:T(8,128)(2,1)S(1)} %copy.45), channel_id=1, replica_groups=mesh['sp_0'=8,'sp_1'=4,'tp'=16] {'sp_1'}, dimensions={0}, use_global_device_ids=true | all-gather | bytes 327680 | tf_op jit(solution)/shard_map/all_gather | solution.py:31
  51.9 0.5 broadcast_select_fusion.3
  52.6 21.8 %all_gather.25 = bf16[8,1,128,256]{3,2,1,0:T(8,128)(2,1)} all-gather(bf16[1,1,128,256]{3,2,1,0:T(8,128)(2,1)S(1)} %fusion.46), channel_id=1, replica_groups=mesh['sp_0'=8,'sp_1'=4,'tp'=16] {'sp_0'}, dimensions={0}, use_global_device_ids=true | all-gather | bytes 589824 | tf_op jit(solution)/shard_map/all_gather | solution.py:31
  74.4 0.6 convert_element_type.645
  74.9 0.5 fusion.4
  75.4 1.9 multiply_reduce_fusion
  77.4 1.7 fusion.29
  79.1 53.5 %all-gather.2.cloned.1.call-done = bf16[256,4096]{1,0:T(8,128)(2,1)} async-done(((bf16[256,256]{1,0:T(8,128)(2,1)}), bf16[256,4096]{1,0:T(8,128)(2,1)}) %all-gather.2.cloned.1.call-update) | async-done | bytes 2097168 | tf_op jit(solution)/shard_map/all_gather | solution.py:168
  132.6 2.3 fusion.6
  134.9 0.6 copy-done.4
  135.5 1.2 broadcast_in_dim.52
  136.7 5.1 %all-to-all-start = ((bf16[16,256,128]{2,1,0:T(8,128)(2,1)}), bf16[16,256,128]{2,1,0:T(8,128)(2,1)S(1)}, u32[]{:S(2)}, u32[]{:S(2)}) async-start(bf16[16,256,128]{2,1,0:T(8,128)(2,1)} %broadcast_in_dim.52), calls=%async_computation | async-start | bytes 2097152 | tf_op jit(solution)/shard_map/all_to_all | solution.py:54
  142.9 0.4 fusion.12
  143.4 26.5 %all-to-all-done = bf16[16,256,128]{2,1,0:T(8,128)(2,1)S(1)} async-done(((bf16[16,256,128]{2,1,0:T(8,128)(2,1)}), bf16[16,256,128]{2,1,0:T(8,128)(2,1)S(1)}, u32[]{:S(2)}, u32[]{:S(2)}) %all-to-all-start) | async-done | bytes 1048608 | tf_op jit(solution)/shard_map/all_to_all | solution.py:54
  169.8 0.3 fusion
  170.1 0.3 fusion.2
  170.5 9.7 %scatter_custom_fusion = bf16[384,512]{1,0:T(8,128)(2,1)S(1)} fusion(s32[1024]{0:T(1024)S(1)} %bitcast.324, bf16[256,512]{1,0:T(8,128)(2,1)S(1)} %constant_dynamic-slice_fusion.2, s32[1024]{0:T(1024)S(1)} %broadcast_clamp_fusion.1, bf16[]{:T(256)} %constant.181.clone.1), kind=kCustom, calls=%fused_computation.26 | custom fusion | bytes 393218 | tf_op jit(solution)/shard_map/scatter | solution.py:207
  180.3 27.1 %all_to_all.15 = bf16[32,12,512]{2,1,0:T(8,128)(2,1)S(1)} all-to-all(bf16[32,12,512]{2,1,0:T(8,128)(2,1)S(1)} %reshape.1386), channel_id=1, replica_groups=mesh['sp_0'=8,'sp_1'=4,'tp'=16] {'sp_0','sp_1'}, dimensions={0} | all-to-all | bytes 786432 | tf_op jit(solution)/shard_map/all_to_all | solution.py:209
  207.4 1.9 collective-permute-start
  209.3 1.9 collective-permute-done
  211.2 0.4 maximum_select_fusion.1
  211.5 1.3 copy.52
  212.9 2.1 collective-permute-start.1
  215.2 1.1 maximum_select_fusion.2
  216.3 17.7 %collective-permute-done.1 = bf16[32,12,1024]{2,0,1:T(8,128)(2,1)} collective-permute-done((bf16[32,12,1024]{2,0,1:T(8,128)(2,1)}, bf16[32,12,1024]{2,0,1:T(8,128)(2,1)}, u32[]{:S(2)}, u32[]{:S(2)}) %collective-permute-start.1) | collective-permute-done | bytes 786464 | tf_op jit(solution)/shard_map/ppermute | solution.py:64
  234.0 1.6 copy.53
  235.6 1.1 concatenate.32
  236.7 2.8 fusion.18
  239.5 5.1 %fusion.19 = f32[384,2048]{1,0:T(8,128)} fusion(bf16[256,2048]{1,0:T(8,128)(2,1)S(1)} %copy-done, f32[384,256]{1,0:T(8,128)S(1)} %fusion.18, bf16[2048,256]{1,0:T(8,128)(2,1)} %param.31, bf16[384,1024]{1,0:T(8,128)(2,1)} %maximum_select_fusion.2, bf16[384,1024]{1,0:T(8,128)(2,1)S(1)} %copy-done.3, pred[]{:T(512)S(6)} %eq.66), kind=kOutput, calls=%fused_computation.48 | convolution fusion | flops 812974080 | bytes 7208961 | tf_op jit(solution)/shard_map/dot_general | solution.py:228
  244.7 5.6 %reshape_reshape.3 = f32[384,4,2,2,128]{4,3,2,1,0:T(2,128)} reshape(f32[384,2048]{1,0:T(8,128)} %fusion.19) | data formatting | bytes 6291456 | tf_op jit(solution)/shard_map/reshape;reshape | solution.py:232
  250.3 1.9 constant_dynamic-slice_fusion
  252.4 2.2 collective-permute-start.2
  254.7 2.0 constant_dynamic-slice_fusion.1
  256.6 15.9 %collective-permute-done.2 = bf16[384,4,2,128]{3,1,0,2:T(4,128)(2,1)} collective-permute-done((bf16[384,4,2,128]{3,1,0,2:T(4,128)(2,1)S(1)}, bf16[384,4,2,128]{3,1,0,2:T(4,128)(2,1)}, u32[]{:S(2)}, u32[]{:S(2)}) %collective-permute-start.2) | collective-permute-done | bytes 786464 | tf_op jit(solution)/shard_map/ppermute | solution.py:64
  272.6 1.7 bitcast_add_fusion
  274.3 1.1 copy-done.1
  275.6 3.8 %collective-permute-start.3 = (bf16[384,4,1,128]{3,1,0,2:T(4,128)(2,1)S(1)}, bf16[384,4,1,128]{3,1,0,2:T(4,128)(2,1)S(1)}, u32[]{:S(2)}, u32[]{:S(2)}) collective-permute-start(bf16[384,4,1,128]{3,1,0,2:T(4,128)(2,1)S(1)} %dynamic-slice_convert_fusion), channel_id=1, source_target_pairs={{0,1},{1,0},{2,3},{3,2},{4,5},{5,4},{6,7},{7,6},{8,9},{9,8},{10,11... | collective-permute-start | bytes 1179656 | tf_op jit(solution)/shard_map/ppermute | solution.py:64
  279.3 1.3 collective-permute-done.3
  280.6 2.1 add_convert_fusion
  282.7 4.3 %all-to-all-start.2 = ((bf16[32,12,4,128]{3,2,1,0:T(4,128)(2,1)}), bf16[32,12,4,128]{3,2,1,0:T(4,128)(2,1)S(1)}, u32[]{:S(2)}, u32[]{:S(2)}) async-start(bf16[32,12,4,128]{3,2,1,0:T(4,128)(2,1)} %bitcast.64), calls=%async_computation.2 | async-start | bytes 786432 | tf_op jit(solution)/shard_map/all_to_all | solution.py:243
  287.1 0.8 copy.56
  287.9 1.0 fusion.143
  289.0 12.0 %all-to-all-done.2 = bf16[32,12,4,128]{3,2,1,0:T(4,128)(2,1)S(1)} async-done(((bf16[32,12,4,128]{3,2,1,0:T(4,128)(2,1)}), bf16[32,12,4,128]{3,2,1,0:T(4,128)(2,1)S(1)}, u32[]{:S(2)}, u32[]{:S(2)}) %all-to-all-start.2) | async-done | bytes 393248 | tf_op jit(solution)/shard_map/all_to_all | solution.py:243
  300.9 3.6 %gather_fusion = bf16[1024,4,128]{2,1,0:T(4,128)(2,1)S(1)} fusion(bf16[384,4,128]{2,1,0:T(4,128)(2,1)S(1)} %bitcast.299, s32[1024]{0:T(1024)S(1)} %broadcast_clamp_fusion), kind=kCustom, calls=%fused_computation.1 | custom fusion | bytes 2101248 | tf_op jit(solution)/shard_map/gather | solution.py:249
  304.5 2.7 fusion.3
  307.4 4.1 %collective-permute-start.4 = (bf16[256,2,128]{2,0,1:T(8,128)(2,1)S(1)}, bf16[256,2,128]{2,0,1:T(8,128)(2,1)S(1)}, u32[]{:S(2)}, u32[]{:S(2)}) collective-permute-start(bf16[256,2,128]{2,0,1:T(8,128)(2,1)S(1)} %fusion.50), channel_id=1, source_target_pairs={{0,8},{1,9},{2,10},{3,11},{4,12},{5,13},{6,14},{7,15},{8,0},{9,1},... | collective-permute-start | bytes 393224 | tf_op jit(solution)/shard_map/ppermute | solution.py:64
  311.6 0.4 fusion.7
  312.0 19.9 %all_gather.27 = bf16[256,512]{0,1:T(8,128)(2,1)S(1)} all-gather(bf16[256,32]{0,1:T(8,128)(2,1)S(1)} %fusion.7), channel_id=1, replica_groups=mesh['sp_0'=8,'sp_1'=4,'tp'=16] {'tp'}, dimensions={1}, use_global_device_ids=true | all-gather | bytes 278528 | tf_op jit(solution)/shard_map/all_gather | solution.py:239
  331.9 1.9 collective-permute-start.5
  333.9 0.3 fusion.144
  334.1 6.0 %collective-permute-done.5 = bf16[256,1,128]{2,0,1:T(8,128)(2,1)S(1)} collective-permute-done((bf16[256,1,128]{2,0,1:T(8,128)(2,1)S(1)}, bf16[256,1,128]{2,0,1:T(8,128)(2,1)S(1)}, u32[]{:S(2)}, u32[]{:S(2)}) %collective-permute-start.5) | collective-permute-done | bytes 65568 | tf_op jit(solution)/shard_map/ppermute | solution.py:64
  340.1 0.7 fusion.66
  (89 shorter events, 2.9 us)
Async XLA Ops:
  6.5 233.0 %copy-start = (bf16[256,2048]{1,0:T(8,128)(2,1)S(1)}, bf16[256,2048]{1,0:T(8,128)(2,1)}, u32[]{:S(2)}) copy-start(bf16[256,2048]{1,0:T(8,128)(2,1)} %param.32) | copy-start | bytes 3145732
  6.5 126.1 %all-gather.2.cloned.1.call-start = ((), (), s32[]{:S(2)}) async-start(), calls=%async_computation.3 | async-start | bytes 2228224 | tf_op jit(solution)/shard_map/all_gather | solution.py:168
  9.9 32.0 %copy-start.12 = (bf16[256,128]{1,0:T(8,128)(2,1)S(1)}, bf16[256,128]{1,0:T(8,128)(2,1)}, u32[]{:S(2)}) copy-start(bf16[256,128]{1,0:T(8,128)(2,1)} %param.18) | copy-start | bytes 196612
  10.2 31.7 %copy-start.7 = (bf16[256,128]{1,0:T(8,128)(2,1)S(1)}, bf16[256,128]{1,0:T(8,128)(2,1)}, u32[]{:S(2)}) copy-start(bf16[256,128]{1,0:T(8,128)(2,1)} %param.19) | copy-start | bytes 196612
  11.6 30.7 %copy-start.6 = (bf16[256,256]{1,0:T(8,128)(2,1)S(1)}, bf16[256,256]{1,0:T(8,128)(2,1)}, u32[]{:S(2)}) copy-start(bf16[256,256]{1,0:T(8,128)(2,1)} %param.20) | copy-start | bytes 393220
  13.3 61.0 %copy-start.18 = (bf16[256]{0:T(256)(128)(2,1)S(1)}, bf16[256]{0:T(256)(128)(2,1)}, u32[]{:S(2)}) copy-start(bf16[256]{0:T(256)(128)(2,1)} %param.24) | copy-start | bytes 1540
  74.9 57.7 %copy-start.2 = (bf16[4096,128]{1,0:T(8,128)(2,1)S(1)}, bf16[4096,128]{1,0:T(8,128)(2,1)}, u32[]{:S(2)}) copy-start(bf16[4096,128]{1,0:T(8,128)(2,1)} %param.25) | copy-start | bytes 3145732
  75.4 2.0 copy-start.17
  75.4 57.2 %copy-start.13 = (bf16[256,128]{1,0:T(8,128)(2,1)S(1)}, bf16[256,128]{1,0:T(8,128)(2,1)}, u32[]{:S(2)}) copy-start(bf16[256,128]{1,0:T(8,128)(2,1)} %param.26) | copy-start | bytes 196612
  134.9 0.6 copy-start.4
  135.5 6.3 %copy-start.14 = (s32[256,4]{0,1:T(4,128)S(1)}, s32[256,4]{0,1:T(4,128)}, u32[]{:S(2)}) copy-start(s32[256,4]{0,1:T(4,128)} %param.28) | copy-start | bytes 12292
  135.5 6.8 %copy-start.16 = (bf16[2048]{0:T(1024)(128)(2,1)S(1)}, bf16[2048]{0:T(1024)(128)(2,1)}, u32[]{:S(2)}) copy-start(bf16[2048]{0:T(1024)(128)(2,1)} %param.27) | copy-start | bytes 12292
  136.7 33.1 %all-to-all-start = ((bf16[16,256,128]{2,1,0:T(8,128)(2,1)}), bf16[16,256,128]{2,1,0:T(8,128)(2,1)S(1)}, u32[]{:S(2)}, u32[]{:S(2)}) async-start(bf16[16,256,128]{2,1,0:T(8,128)(2,1)} %broadcast_in_dim.52), calls=%async_computation | async-start | bytes 2097152 | tf_op jit(solution)/shard_map/all_to_all | solution.py:54
  207.4 3.8 %collective-permute-start = (bf16[32,12,512]{2,1,0:T(8,128)(2,1)S(1)}, bf16[32,12,512]{2,1,0:T(8,128)(2,1)S(1)}, u32[]{:S(2)}, u32[]{:S(2)}) collective-permute-start(bf16[32,12,512]{2,1,0:T(8,128)(2,1)S(1)} %all_to_all.15), channel_id=1, source_target_pairs={{0,1},{1,0},{2,3},{3,2},{4,5},{5,4},{6,7},{7,6},{8,9},{9,8},{10,11... | collective-permute-start | bytes 1179656 | tf_op jit(solution)/shard_map/ppermute | solution.py:64
  212.9 21.2 %collective-permute-start.1 = (bf16[32,12,1024]{2,0,1:T(8,128)(2,1)}, bf16[32,12,1024]{2,0,1:T(8,128)(2,1)}, u32[]{:S(2)}, u32[]{:S(2)}) collective-permute-start(bf16[32,12,1024]{2,0,1:T(8,128)(2,1)} %copy.52), channel_id=1, source_target_pairs={{0,2},{1,3},{2,0},{3,1},{4,6},{5,7},{6,4},{7,5},{8,10},{9,11},{10,... | collective-permute-start | bytes 2359304 | tf_op jit(solution)/shard_map/ppermute | solution.py:64
  236.7 2.8 copy-start.3
  252.4 20.1 %collective-permute-start.2 = (bf16[384,4,2,128]{3,1,0,2:T(4,128)(2,1)S(1)}, bf16[384,4,2,128]{3,1,0,2:T(4,128)(2,1)}, u32[]{:S(2)}, u32[]{:S(2)}) collective-permute-start(bf16[384,4,2,128]{3,1,0,2:T(4,128)(2,1)S(1)} %bitcast.308), channel_id=1, source_target_pairs={{0,2},{1,3},{2,0},{3,1},{4,6},{5,7},{6,4},{7,5},{8,10},{9,11},{10,... | collective-permute-start | bytes 2359304 | tf_op jit(solution)/shard_map/ppermute | solution.py:64
  274.3 1.1 copy-start.1
  275.4 11.7 %copy-start.15 = (f32[256,4]{0,1:T(4,128)S(1)}, f32[256,4]{0,1:T(4,128)}, u32[]{:S(2)}) copy-start(f32[256,4]{0,1:T(4,128)} %param.29) | copy-start | bytes 12292
  275.4 12.5 %copy-start.8 = (bf16[2048,32]{0,1:T(8,128)(2,1)S(1)}, bf16[2048,32]{0,1:T(8,128)(2,1)}, u32[]{:S(2)}) copy-start(bf16[2048,32]{0,1:T(8,128)(2,1)} %param.33) | copy-start | bytes 393220
  275.6 5.1 %collective-permute-start.3 = (bf16[384,4,1,128]{3,1,0,2:T(4,128)(2,1)S(1)}, bf16[384,4,1,128]{3,1,0,2:T(4,128)(2,1)S(1)}, u32[]{:S(2)}, u32[]{:S(2)}) collective-permute-start(bf16[384,4,1,128]{3,1,0,2:T(4,128)(2,1)S(1)} %dynamic-slice_convert_fusion), channel_id=1, source_target_pairs={{0,1},{1,0},{2,3},{3,2},{4,5},{5,4},{6,7},{7,6},{8,9},{9,8},{10,11... | collective-permute-start | bytes 1179656 | tf_op jit(solution)/shard_map/ppermute | solution.py:64
  282.7 18.2 %all-to-all-start.2 = ((bf16[32,12,4,128]{3,2,1,0:T(4,128)(2,1)}), bf16[32,12,4,128]{3,2,1,0:T(4,128)(2,1)S(1)}, u32[]{:S(2)}, u32[]{:S(2)}) async-start(bf16[32,12,4,128]{3,2,1,0:T(4,128)(2,1)} %bitcast.64), calls=%async_computation.2 | async-start | bytes 786432 | tf_op jit(solution)/shard_map/all_to_all | solution.py:243
  304.5 7.0 %copy-start.9 = (bf16[2048,32]{0,1:T(8,128)(2,1)S(1)}, bf16[2048,32]{0,1:T(8,128)(2,1)}, u32[]{:S(2)}) copy-start(bf16[2048,32]{0,1:T(8,128)(2,1)} %param.34) | copy-start | bytes 393220
  304.5 7.0 %copy-start.10 = (f32[256,32]{0,1:T(8,128)S(1)}, f32[256,32]{0,1:T(8,128)}, u32[]{:S(2)}) copy-start(f32[256,32]{0,1:T(8,128)} %fusion.143) | copy-start | bytes 98308
  307.3 26.6 %copy-start.11 = (bf16[512,128]{1,0:T(8,128)(2,1)S(1)}, bf16[512,128]{1,0:T(8,128)(2,1)}, u32[]{:S(2)}) copy-start(bf16[512,128]{1,0:T(8,128)(2,1)} %param.35) | copy-start | bytes 393220
  307.3 32.8 %copy-start.5 = (bf16[256,128]{1,0:T(8,128)(2,1)S(1)}, bf16[256,128]{1,0:T(8,128)(2,1)}, u32[]{:S(2)}) copy-start(bf16[256,128]{1,0:T(8,128)(2,1)} %copy-done.4) | copy-start | bytes 196612
  307.4 24.5 %collective-permute-start.4 = (bf16[256,2,128]{2,0,1:T(8,128)(2,1)S(1)}, bf16[256,2,128]{2,0,1:T(8,128)(2,1)S(1)}, u32[]{:S(2)}, u32[]{:S(2)}) collective-permute-start(bf16[256,2,128]{2,0,1:T(8,128)(2,1)S(1)} %fusion.50), channel_id=1, source_target_pairs={{0,8},{1,9},{2,10},{3,11},{4,12},{5,13},{6,14},{7,15},{8,0},{9,1},... | collective-permute-start | bytes 393224 | tf_op jit(solution)/shard_map/ppermute | solution.py:64
  331.9 8.2 %collective-permute-start.5 = (bf16[256,1,128]{2,0,1:T(8,128)(2,1)S(1)}, bf16[256,1,128]{2,0,1:T(8,128)(2,1)S(1)}, u32[]{:S(2)}, u32[]{:S(2)}) collective-permute-start(bf16[256,1,128]{2,0,1:T(8,128)(2,1)S(1)} %dynamic-slice_convert_fusion.2), channel_id=1, source_target_pairs={{0,4},{1,5},{2,6},{3,7},{4,0},{5,1},{6,2},{7,3},{8,12},{9,13},{10,... | collective-permute-start | bytes 196616 | tf_op jit(solution)/shard_map/ppermute | solution.py:64
Sparse Core Ops, SparseCore 0:
  79.2 53.3 all-gather.1
where the time goes:
time: 349 us; the launch traced here: 348 us
  waiting for transfers between devices  135 us (39%)
  blocking collectives  105 us (30%)
  local copies, waits for them, and re-layouts  33.1 us (9%)
  starting transfers between devices  25.5 us (7%)
  matrix products  18 us (5%)
  other arithmetic  16.9 us (5%)
  between operations  14.1 us (4%)
    all_gather x4, blocking collectives, prefix_by_axis(): lax.all_gather(part.astype(kind), axis)  58.2 us
    all_gather x1, waiting for transfers between devices, body(): lax.all_gather(head_rows, 'tp', axis=1, tiled=True)  53.5 us
    ppermute x6, waiting for transfers between devices, from_partner(): return lax.ppermute(value, axis, pairs)  42.8 us
    all_to_all x1, blocking collectives, body(): lax.all_to_all(outgoing.reshape(senders, rows_most, part_width), SP, spli...  27.1 us
    all_to_all x1, waiting for transfers between devices, sent_to_all(): return lax.all_to_all(copies, axis, split_axis=0, concat_axis=0, tiled=True)  26.5 us
    all_gather x1, blocking collectives, body(): lax.all_gather(shared_hidden, 'tp', axis=1, tiled=True)  19.9 us
    ppermute x6, starting transfers between devices, from_partner(): return lax.ppermute(value, axis, pairs)  16.1 us
    all_to_all x1, waiting for transfers between devices, body(): lax.all_to_all(expert_out, SP, split_axis=0, concat_axis=0, tiled=True)  12 us
  transfers between devices with their start and end apart: 9, of which 8 were waited for; matrix products, arithmetic and copies ran while one was open for 2% of the time, Pallas kernels for 0%

commit v1 on v0

--- a/solution.py
+++ b/solution.py
@@ -14,6 +14,27 @@
 EPSILON = 1e-06
 ROUTE_SCALE = 2.5
 GATE_TEMPER = 16.0
+
+
+def collect(x, axis, dim):
+    peers, index, rows = (lax.axis_size(axis), lax.axis_index(axis), x.shape[dim])
+    right = [(i, (i + 1) % peers) for i in range(peers)]
+    left = [(i, (i - 1) % peers) for i in range(peers)]
+    result = jnp.zeros((*x.shape[:dim], peers * rows, *x.shape[dim + 1 :]), x.dtype)
+    result = lax.dynamic_update_slice_in_dim(result, x, index * rows, axis=dim)
+    from_left = from_right = x
+    halfway = peers // 2
+    for step in range(1, halfway + 1):
+        from_left = lax.ppermute(from_left, axis, right)
+        result = lax.dynamic_update_slice_in_dim(
+            result, from_left, (index - step) % peers * rows, axis=dim
+        )
+        if step < peers - halfway:
+            from_right = lax.ppermute(from_right, axis, left)
+            result = lax.dynamic_update_slice_in_dim(
+                result, from_right, (index + step) % peers * rows, axis=dim
+            )
+    return result
 
 
 def nothing_yet(value, identity):
@@ -165,9 +186,7 @@
         .astype(jnp.bfloat16)
     )
     projected = jnp.dot(
-        lax.all_gather(head_rows, "tp", axis=1, tiled=True),
-        output_projection,
-        preferred_element_type=jnp.float32,
+        collect(head_rows, "tp", 1), output_projection, preferred_element_type=jnp.float32
     )
     mid_local = (residual.astype(jnp.float32) + projected).astype(jnp.bfloat16)
     mid_rows = gather_directly(mid_local, "tp", 1).astype(jnp.float32)

time: 349 us -> 330 us (0.946)
  starting transfers between devices: 25.5 us -> 72.8 us
  waiting for transfers between devices: 135 us -> 96.1 us
  between operations: 14.1 us -> 0.89 us
  blocking collectives: 105 us -> 96.7 us
    all_gather x1 -> x0, waiting for transfers between devices: 53.5 us -> none  [body(): lax.all_gather(head_rows, 'tp', axis=1, tiled=True)]
    ppermute x0 -> x15, starting transfers between devices: none -> 40.5 us  [the longest x8 24.8 us: collect(): from_left = lax.ppermute(from_left, axis, right)]
    ppermute x0 -> x15, waiting for transfers between devices: none -> 14.9 us  [the longest x8 13.5 us: collect(): from_left = lax.ppermute(from_left, axis, right)]
    all_to_all x1, starting transfers between devices: 5.14 us -> 11.9 us  [sent_to_all(): return lax.all_to_all(copies, axis, split_axis=0, concat_axis=0, tiled=True)]
    all_to_all x1, blocking collectives: 27.1 us -> 20.8 us  [body(): lax.all_to_all(outgoing.reshape(senders, rows_most, part_width), SP, spli...]
  transfers between devices with their start and end apart: 9 -> 23, of which waited for: 8 -> 21; matrix products, arithmetic and copies ran while one was open for 2% -> 2% of each run, Pallas kernels for 0% -> 0%
where the time goes in v1:
time: 330 us; the launch traced here: 329 us
  blocking collectives  96.7 us (29%)
  waiting for transfers between devices  96.1 us (29%)
  starting transfers between devices  72.8 us (22%)
  local copies, waits for them, and re-layouts  33.6 us (10%)
  matrix products  15.3 us (5%)
  other arithmetic  13.8 us (4%)
    all_gather x4, blocking collectives, prefix_by_axis(): lax.all_gather(part.astype(kind), axis)  56 us
    ppermute x6, waiting for transfers between devices, from_partner(): return lax.ppermute(value, axis, pairs)  42.8 us
    all_to_all x1, waiting for transfers between devices, sent_to_all(): return lax.all_to_all(copies, axis, split_axis=0, concat_axis=0, tiled=True)  26.5 us
    ppermute x8, starting transfers between devices, collect(): from_left = lax.ppermute(from_left, axis, right)  24.8 us
    all_to_all x1, blocking collectives, body(): lax.all_to_all(outgoing.reshape(senders, rows_most, part_width), SP, spli...  20.8 us
    all_gather x1, blocking collectives, body(): lax.all_gather(shared_hidden, 'tp', axis=1, tiled=True)  19.9 us
    ppermute x6, starting transfers between devices, from_partner(): return lax.ppermute(value, axis, pairs)  16.1 us
    ppermute x7, starting transfers between devices, collect(): from_right = lax.ppermute(from_right, axis, left)  15.7 us
  transfers between devices with their start and end apart: 23, of which 21 were waited for; matrix products, arithmetic and copies ran while one was open for 2% of the time, Pallas kernels for 0%

profile of v1, /device:TPU:1, one launch (start us, length us, event | category | flops | bytes accessed | tf_op | source)
XLA Modules:
  0.0 329.2 jit_solution(1025911323187193486)
XLA Ops:
  0.0 1.0 fusion.52
  1.6 1.3 reduce.7
  3.7 1.4 fusion.49
  5.1 1.7 convolution_bitcast_fusion
  7.0 8.5 %all_gather.19 = bf16[4,1,128]{2,1,0:T(2,128)(2,1)S(1)} all-gather(bf16[1,1,128]{2,1,0:T(2,128)(2,1)S(1)} %get-tuple-element.7), channel_id=1, replica_groups=mesh['sp_0'=8,'sp_1'=4,'tp'=16] {'sp_1'}, dimensions={0}, use_global_device_ids=true | all-gather | bytes 1280 | tf_op jit(solution)/shard_map/all_gather | solution.py:52
  15.6 18.6 %all_gather.20 = bf16[8,1,128]{2,1,0:T(2,128)(2,1)S(1)} all-gather(bf16[1,1,128]{2,1,0:T(2,128)(2,1)S(1)} %multiply_convert_fusion.1), channel_id=1, replica_groups=mesh['sp_0'=8,'sp_1'=4,'tp'=16] {'sp_0'}, dimensions={0}, use_global_device_ids=true | all-gather | bytes 2304 | tf_op jit(solution)/shard_map/all_gather | solution.py:52
  34.9 9.4 %all_gather.21 = bf16[4,1,128,256]{3,2,1,0:T(8,128)(2,1)S(1)} all-gather(bf16[1,1,128,256]{3,2,1,0:T(8,128)(2,1)S(1)} %copy.45), channel_id=1, replica_groups=mesh['sp_0'=8,'sp_1'=4,'tp'=16] {'sp_1'}, dimensions={0}, use_global_device_ids=true | all-gather | bytes 327680 | tf_op jit(solution)/shard_map/all_gather | solution.py:52
  44.4 19.5 %all_gather.22 = bf16[8,1,128,256]{3,2,1,0:T(8,128)(2,1)S(1)} all-gather(bf16[1,1,128,256]{3,2,1,0:T(8,128)(2,1)S(1)} %fusion.46), channel_id=1, replica_groups=mesh['sp_0'=8,'sp_1'=4,'tp'=16] {'sp_0'}, dimensions={0}, use_global_device_ids=true | all-gather | bytes 589824 | tf_op jit(solution)/shard_map/all_gather | solution.py:52
  64.5 0.8 multiply_reduce_fusion
  65.6 0.8 constant_dynamic-update-slice_fusion.15
  66.4 16.6 %collective-permute-start = (bf16[256,256]{1,0:T(8,128)(2,1)}, bf16[256,256]{1,0:T(8,128)(2,1)S(1)}, u32[]{:S(2)}, u32[]{:S(2)}) collective-permute-start(bf16[256,256]{1,0:T(8,128)(2,1)} %get-tuple-element.26), channel_id=1, source_target_pairs={{0,1},{1,2},{2,3},{3,4},{4,5},{5,6},{6,7},{7,8},{8,9},{9,10},{10,1... | collective-permute-start | bytes 393224 | tf_op jit(solution)/shard_map/ppermute | solution.py:28
  83.0 2.3 collective-permute-done
  85.3 2.3 collective-permute-start.2
  87.7 1.9 collective-permute-done.2
  89.6 2.4 collective-permute-start.4
  92.3 0.9 collective-permute-start.5
  93.3 0.8 collective-permute-done.4
  94.1 2.3 collective-permute-start.6
  96.7 2.2 collective-permute-start.7
  98.9 0.8 collective-permute-done.6
  99.7 1.1 collective-permute-start.8
  101.1 3.4 %collective-permute-start.9 = (bf16[256,256]{1,0:T(8,128)(2,1)S(1)}, bf16[256,256]{1,0:T(8,128)(2,1)S(1)}, u32[]{:S(2)}, u32[]{:S(2)}) collective-permute-start(bf16[256,256]{1,0:T(8,128)(2,1)S(1)} %collective-permute-done.7), channel_id=1, source_target_pairs={{0,15},{1,0},{2,1},{3,2},{4,3},{5,4},{6,5},{7,6},{8,7},{9,8},{10,9... | collective-permute-start | bytes 393224 | tf_op jit(solution)/shard_map/ppermute | solution.py:33
  104.5 0.8 collective-permute-done.8
  105.5 4.6 %collective-permute-start.11 = (bf16[256,256]{1,0:T(8,128)(2,1)S(1)}, bf16[256,256]{1,0:T(8,128)(2,1)S(1)}, u32[]{:S(2)}, u32[]{:S(2)}) collective-permute-start(bf16[256,256]{1,0:T(8,128)(2,1)S(1)} %collective-permute-done.9), channel_id=1, source_target_pairs={{0,15},{1,0},{2,1},{3,2},{4,3},{5,4},{6,5},{7,6},{8,7},{9,8},{10,9... | collective-permute-start | bytes 393224 | tf_op jit(solution)/shard_map/ppermute | solution.py:33
  110.1 0.8 collective-permute-done.10
  111.0 4.6 %collective-permute-start.13 = (bf16[256,256]{1,0:T(8,128)(2,1)S(1)}, bf16[256,256]{1,0:T(8,128)(2,1)S(1)}, u32[]{:S(2)}, u32[]{:S(2)}) collective-permute-start(bf16[256,256]{1,0:T(8,128)(2,1)S(1)} %collective-permute-done.11), channel_id=1, source_target_pairs={{0,15},{1,0},{2,1},{3,2},{4,3},{5,4},{6,5},{7,6},{8,7},{9,8},{10,9... | collective-permute-start | bytes 393224 | tf_op jit(solution)/shard_map/ppermute | solution.py:33
  115.7 0.8 collective-permute-done.12
  116.7 5.4 %collective-permute-done.14 = bf16[256,256]{1,0:T(8,128)(2,1)S(1)} collective-permute-done((bf16[256,256]{1,0:T(8,128)(2,1)S(1)}, bf16[256,256]{1,0:T(8,128)(2,1)S(1)}, u32[]{:S(2)}, u32[]{:S(2)}) %collective-permute-start.14) | collective-permute-done | bytes 131104 | tf_op jit(solution)/shard_map/ppermute | solution.py:28
  122.1 0.7 fusion.6
  123.5 1.2 broadcast_in_dim.91
  124.7 11.9 %all-to-all-start = ((bf16[16,256,128]{2,1,0:T(8,128)(2,1)}), bf16[16,256,128]{2,1,0:T(8,128)(2,1)S(1)}, u32[]{:S(2)}, u32[]{:S(2)}) async-start(bf16[16,256,128]{2,1,0:T(8,128)(2,1)} %broadcast_in_dim.91), calls=%async_computation | async-start | bytes 2097152 | tf_op jit(solution)/shard_map/all_to_all | solution.py:75
  138.1 26.5 %all-to-all-done = bf16[16,256,128]{2,1,0:T(8,128)(2,1)S(1)} async-done(((bf16[16,256,128]{2,1,0:T(8,128)(2,1)}), bf16[16,256,128]{2,1,0:T(8,128)(2,1)S(1)}, u32[]{:S(2)}, u32[]{:S(2)}) %all-to-all-start) | async-done | bytes 1048608 | tf_op jit(solution)/shard_map/all_to_all | solution.py:75
  165.2 9.7 %scatter_custom_fusion = bf16[384,512]{1,0:T(8,128)(2,1)S(1)} fusion(s32[1024]{0:T(1024)S(1)} %bitcast.324, bf16[256,512]{1,0:T(8,128)(2,1)S(1)} %constant_dynamic-slice_fusion.2, s32[1024]{0:T(1024)S(1)} %broadcast_clamp_fusion.1, bf16[]{:T(256)} %constant.237.clone.1), kind=kCustom, calls=%fused_computation.26 | custom fusion | bytes 393218 | tf_op jit(solution)/shard_map/scatter | solution.py:226
  175.0 20.8 %all_to_all.15 = bf16[32,12,512]{2,1,0:T(8,128)(2,1)S(1)} all-to-all(bf16[32,12,512]{2,1,0:T(8,128)(2,1)S(1)} %reshape.1386), channel_id=1, replica_groups=mesh['sp_0'=8,'sp_1'=4,'tp'=16] {'sp_0','sp_1'}, dimensions={0} | all-to-all | bytes 786432 | tf_op jit(solution)/shard_map/all_to_all | solution.py:228
  195.8 1.9 collective-permute-start.15
  197.7 1.9 collective-permute-done.15
  200.0 1.3 copy.52
  201.3 2.1 collective-permute-start.16
  203.6 1.1 maximum_select_fusion.2
  204.8 17.7 %collective-permute-done.16 = bf16[32,12,1024]{2,0,1:T(8,128)(2,1)} collective-permute-done((bf16[32,12,1024]{2,0,1:T(8,128)(2,1)}, bf16[32,12,1024]{2,0,1:T(8,128)(2,1)}, u32[]{:S(2)}, u32[]{:S(2)}) %collective-permute-start.16) | collective-permute-done | bytes 786464 | tf_op jit(solution)/shard_map/ppermute | solution.py:85
  222.5 1.6 copy.53
  224.0 1.1 concatenate.32
  225.1 2.8 fusion.18
  227.9 5.2 %fusion.19 = f32[384,2048]{1,0:T(8,128)} fusion(bf16[256,2048]{1,0:T(8,128)(2,1)S(1)} %copy-done, f32[384,256]{1,0:T(8,128)S(1)} %fusion.18, bf16[2048,256]{1,0:T(8,128)(2,1)} %param.31, bf16[384,1024]{1,0:T(8,128)(2,1)} %maximum_select_fusion.2, bf16[384,1024]{1,0:T(8,128)(2,1)S(1)} %copy-done.3, pred[]{:T(512)S(6)} %eq.81), kind=kOutput, calls=%fused_computation.48 | convolution fusion | flops 812974080 | bytes 7208961 | tf_op jit(solution)/shard_map/dot_general | solution.py:247
  233.1 5.6 %reshape_reshape.3 = f32[384,4,2,2,128]{4,3,2,1,0:T(2,128)} reshape(f32[384,2048]{1,0:T(8,128)} %fusion.19) | data formatting | bytes 6291456 | tf_op jit(solution)/shard_map/reshape;reshape | solution.py:251
  238.7 1.9 constant_dynamic-slice_fusion
  240.9 2.2 collective-permute-start.17
  243.1 2.0 constant_dynamic-slice_fusion.1
  245.1 15.9 %collective-permute-done.17 = bf16[384,4,2,128]{3,1,0,2:T(4,128)(2,1)} collective-permute-done((bf16[384,4,2,128]{3,1,0,2:T(4,128)(2,1)S(1)}, bf16[384,4,2,128]{3,1,0,2:T(4,128)(2,1)}, u32[]{:S(2)}, u32[]{:S(2)}) %collective-permute-start.17) | collective-permute-done | bytes 786464 | tf_op jit(solution)/shard_map/ppermute | solution.py:85
  261.0 1.7 bitcast_add_fusion
  262.7 1.2 copy-done.1
  264.0 3.8 %collective-permute-start.18 = (bf16[384,4,1,128]{3,1,0,2:T(4,128)(2,1)S(1)}, bf16[384,4,1,128]{3,1,0,2:T(4,128)(2,1)S(1)}, u32[]{:S(2)}, u32[]{:S(2)}) collective-permute-start(bf16[384,4,1,128]{3,1,0,2:T(4,128)(2,1)S(1)} %dynamic-slice_convert_fusion), channel_id=1, source_target_pairs={{0,1},{1,0},{2,3},{3,2},{4,5},{5,4},{6,7},{7,6},{8,9},{9,8},{10,11... | collective-permute-start | bytes 1179656 | tf_op jit(solution)/shard_map/ppermute | solution.py:85
  267.8 1.3 collective-permute-done.18
  269.1 2.1 add_convert_fusion
  271.2 4.3 %all-to-all-start.2 = ((bf16[32,12,4,128]{3,2,1,0:T(4,128)(2,1)}), bf16[32,12,4,128]{3,2,1,0:T(4,128)(2,1)S(1)}, u32[]{:S(2)}, u32[]{:S(2)}) async-start(bf16[32,12,4,128]{3,2,1,0:T(4,128)(2,1)} %bitcast.64), calls=%async_computation.2 | async-start | bytes 786432 | tf_op jit(solution)/shard_map/all_to_all | solution.py:262
  275.6 0.8 copy.56
  276.4 1.0 fusion.143
  277.4 12.0 %all-to-all-done.2 = bf16[32,12,4,128]{3,2,1,0:T(4,128)(2,1)S(1)} async-done(((bf16[32,12,4,128]{3,2,1,0:T(4,128)(2,1)}), bf16[32,12,4,128]{3,2,1,0:T(4,128)(2,1)S(1)}, u32[]{:S(2)}, u32[]{:S(2)}) %all-to-all-start.2) | async-done | bytes 393248 | tf_op jit(solution)/shard_map/all_to_all | solution.py:262
  289.4 3.6 %gather_fusion = bf16[1024,4,128]{2,1,0:T(4,128)(2,1)S(1)} fusion(bf16[384,4,128]{2,1,0:T(4,128)(2,1)S(1)} %bitcast.299, s32[1024]{0:T(1024)S(1)} %broadcast_clamp_fusion), kind=kCustom, calls=%fused_computation.1 | custom fusion | bytes 2101248 | tf_op jit(solution)/shard_map/gather | solution.py:268
  293.0 2.7 fusion.3
  295.9 4.1 %collective-permute-start.19 = (bf16[256,2,128]{2,0,1:T(8,128)(2,1)S(1)}, bf16[256,2,128]{2,0,1:T(8,128)(2,1)S(1)}, u32[]{:S(2)}, u32[]{:S(2)}) collective-permute-start(bf16[256,2,128]{2,0,1:T(8,128)(2,1)S(1)} %fusion.50), channel_id=1, source_target_pairs={{0,8},{1,9},{2,10},{3,11},{4,12},{5,13},{6,14},{7,15},{8,0},{9,1},... | collective-permute-start | bytes 393224 | tf_op jit(solution)/shard_map/ppermute | solution.py:85
  300.5 19.9 %all_gather.23 = bf16[256,512]{0,1:T(8,128)(2,1)S(1)} all-gather(bf16[256,32]{0,1:T(8,128)(2,1)S(1)} %fusion.7), channel_id=1, replica_groups=mesh['sp_0'=8,'sp_1'=4,'tp'=16] {'tp'}, dimensions={1}, use_global_device_ids=true | all-gather | bytes 278528 | tf_op jit(solution)/shard_map/all_gather | solution.py:258
  320.4 1.9 collective-permute-start.20
  322.6 6.0 %collective-permute-done.20 = bf16[256,1,128]{2,0,1:T(8,128)(2,1)S(1)} collective-permute-done((bf16[256,1,128]{2,0,1:T(8,128)(2,1)S(1)}, bf16[256,1,128]{2,0,1:T(8,128)(2,1)S(1)}, u32[]{:S(2)}, u32[]{:S(2)}) %collective-permute-start.20) | collective-permute-done | bytes 65568 | tf_op jit(solution)/shard_map/ppermute | solution.py:85
  (132 shorter events, 9.9 us)
Async XLA Ops:
  0.0 227.9 %copy-start = (bf16[256,2048]{1,0:T(8,128)(2,1)S(1)}, bf16[256,2048]{1,0:T(8,128)(2,1)}, u32[]{:S(2)}) copy-start(bf16[256,2048]{1,0:T(8,128)(2,1)} %param.32) | copy-start | bytes 3145732
  3.3 30.8 %copy-start.18 = (bf16[256]{0:T(256)(128)(2,1)S(1)}, bf16[256]{0:T(256)(128)(2,1)}, u32[]{:S(2)}) copy-start(bf16[256]{0:T(256)(128)(2,1)} %param.24) | copy-start | bytes 1540
  3.3 30.9 %copy-start.13 = (bf16[256,128]{1,0:T(8,128)(2,1)S(1)}, bf16[256,128]{1,0:T(8,128)(2,1)}, u32[]{:S(2)}) copy-start(bf16[256,128]{1,0:T(8,128)(2,1)} %param.18) | copy-start | bytes 196612
  3.7 30.6 %copy-start.7 = (bf16[256,128]{1,0:T(8,128)(2,1)S(1)}, bf16[256,128]{1,0:T(8,128)(2,1)}, u32[]{:S(2)}) copy-start(bf16[256,128]{1,0:T(8,128)(2,1)} %param.19) | copy-start | bytes 196612
  5.1 29.5 %copy-start.6 = (bf16[256,256]{1,0:T(8,128)(2,1)S(1)}, bf16[256,256]{1,0:T(8,128)(2,1)}, u32[]{:S(2)}) copy-start(bf16[256,256]{1,0:T(8,128)(2,1)} %param.20) | copy-start | bytes 393220
  64.4 1.1 copy-start.11
  66.4 18.9 %collective-permute-start = (bf16[256,256]{1,0:T(8,128)(2,1)}, bf16[256,256]{1,0:T(8,128)(2,1)S(1)}, u32[]{:S(2)}, u32[]{:S(2)}) collective-permute-start(bf16[256,256]{1,0:T(8,128)(2,1)} %get-tuple-element.26), channel_id=1, source_target_pairs={{0,1},{1,2},{2,3},{3,4},{4,5},{5,6},{6,7},{7,8},{8,9},{9,10},{10,1... | collective-permute-start | bytes 393224 | tf_op jit(solution)/shard_map/ppermute | solution.py:28
  83.0 4.6 %collective-permute-start.1 = (bf16[256,256]{1,0:T(8,128)(2,1)}, bf16[256,256]{1,0:T(8,128)(2,1)S(1)}, u32[]{:S(2)}, u32[]{:S(2)}) collective-permute-start(bf16[256,256]{1,0:T(8,128)(2,1)} %get-tuple-element.26), channel_id=1, source_target_pairs={{0,15},{1,0},{2,1},{3,2},{4,3},{5,4},{6,5},{7,6},{8,7},{9,8},{10,9... | collective-permute-start | bytes 393224 | tf_op jit(solution)/shard_map/ppermute | solution.py:33
  83.0 39.1 %copy-start.14 = (bf16[256,128]{1,0:T(8,128)(2,1)S(1)}, bf16[256,128]{1,0:T(8,128)(2,1)}, u32[]{:S(2)}) copy-start(bf16[256,128]{1,0:T(8,128)(2,1)} %param.26) | copy-start | bytes 196612
  83.0 39.1 %copy-start.2 = (bf16[4096,128]{1,0:T(8,128)(2,1)S(1)}, bf16[4096,128]{1,0:T(8,128)(2,1)}, u32[]{:S(2)}) copy-start(bf16[4096,128]{1,0:T(8,128)(2,1)} %param.25) | copy-start | bytes 3145732
  85.3 4.3 %collective-permute-start.2 = (bf16[256,256]{1,0:T(8,128)(2,1)S(1)}, bf16[256,256]{1,0:T(8,128)(2,1)S(1)}, u32[]{:S(2)}, u32[]{:S(2)}) collective-permute-start(bf16[256,256]{1,0:T(8,128)(2,1)S(1)} %collective-permute-done), channel_id=1, source_target_pairs={{0,1},{1,2},{2,3},{3,4},{4,5},{5,6},{6,7},{7,8},{8,9},{9,10},{10,1... | collective-permute-start | bytes 393224 | tf_op jit(solution)/shard_map/ppermute | solution.py:28
  87.6 4.7 %collective-permute-start.3 = (bf16[256,256]{1,0:T(8,128)(2,1)S(1)}, bf16[256,256]{1,0:T(8,128)(2,1)S(1)}, u32[]{:S(2)}, u32[]{:S(2)}) collective-permute-start(bf16[256,256]{1,0:T(8,128)(2,1)S(1)} %collective-permute-done.1), channel_id=1, source_target_pairs={{0,15},{1,0},{2,1},{3,2},{4,3},{5,4},{6,5},{7,6},{8,7},{9,8},{10,9... | collective-permute-start | bytes 393224 | tf_op jit(solution)/shard_map/ppermute | solution.py:33
  89.6 4.5 %collective-permute-start.4 = (bf16[256,256]{1,0:T(8,128)(2,1)S(1)}, bf16[256,256]{1,0:T(8,128)(2,1)S(1)}, u32[]{:S(2)}, u32[]{:S(2)}) collective-permute-start(bf16[256,256]{1,0:T(8,128)(2,1)S(1)} %collective-permute-done.2), channel_id=1, source_target_pairs={{0,1},{1,2},{2,3},{3,4},{4,5},{5,6},{6,7},{7,8},{8,9},{9,10},{10,1... | collective-permute-start | bytes 393224 | tf_op jit(solution)/shard_map/ppermute | solution.py:28
  92.3 4.4 %collective-permute-start.5 = (bf16[256,256]{1,0:T(8,128)(2,1)S(1)}, bf16[256,256]{1,0:T(8,128)(2,1)S(1)}, u32[]{:S(2)}, u32[]{:S(2)}) collective-permute-start(bf16[256,256]{1,0:T(8,128)(2,1)S(1)} %collective-permute-done.3), channel_id=1, source_target_pairs={{0,15},{1,0},{2,1},{3,2},{4,3},{5,4},{6,5},{7,6},{8,7},{9,8},{10,9... | collective-permute-start | bytes 393224 | tf_op jit(solution)/shard_map/ppermute | solution.py:33
  94.1 5.6 %collective-permute-start.6 = (bf16[256,256]{1,0:T(8,128)(2,1)S(1)}, bf16[256,256]{1,0:T(8,128)(2,1)S(1)}, u32[]{:S(2)}, u32[]{:S(2)}) collective-permute-start(bf16[256,256]{1,0:T(8,128)(2,1)S(1)} %collective-permute-done.4), channel_id=1, source_target_pairs={{0,1},{1,2},{2,3},{3,4},{4,5},{5,6},{6,7},{7,8},{8,9},{9,10},{10,1... | collective-permute-start | bytes 393224 | tf_op jit(solution)/shard_map/ppermute | solution.py:28
  96.7 4.4 %collective-permute-start.7 = (bf16[256,256]{1,0:T(8,128)(2,1)S(1)}, bf16[256,256]{1,0:T(8,128)(2,1)S(1)}, u32[]{:S(2)}, u32[]{:S(2)}) collective-permute-start(bf16[256,256]{1,0:T(8,128)(2,1)S(1)} %collective-permute-done.5), channel_id=1, source_target_pairs={{0,15},{1,0},{2,1},{3,2},{4,3},{5,4},{6,5},{7,6},{8,7},{9,8},{10,9... | collective-permute-start | bytes 393224 | tf_op jit(solution)/shard_map/ppermute | solution.py:33
  99.7 5.6 %collective-permute-start.8 = (bf16[256,256]{1,0:T(8,128)(2,1)S(1)}, bf16[256,256]{1,0:T(8,128)(2,1)S(1)}, u32[]{:S(2)}, u32[]{:S(2)}) collective-permute-start(bf16[256,256]{1,0:T(8,128)(2,1)S(1)} %collective-permute-done.6), channel_id=1, source_target_pairs={{0,1},{1,2},{2,3},{3,4},{4,5},{5,6},{6,7},{7,8},{8,9},{9,10},{10,1... | collective-permute-start | bytes 393224 | tf_op jit(solution)/shard_map/ppermute | solution.py:28
  101.1 4.4 %collective-permute-start.9 = (bf16[256,256]{1,0:T(8,128)(2,1)S(1)}, bf16[256,256]{1,0:T(8,128)(2,1)S(1)}, u32[]{:S(2)}, u32[]{:S(2)}) collective-permute-start(bf16[256,256]{1,0:T(8,128)(2,1)S(1)} %collective-permute-done.7), channel_id=1, source_target_pairs={{0,15},{1,0},{2,1},{3,2},{4,3},{5,4},{6,5},{7,6},{8,7},{9,8},{10,9... | collective-permute-start | bytes 393224 | tf_op jit(solution)/shard_map/ppermute | solution.py:33
  105.3 5.6 %collective-permute-start.10 = (bf16[256,256]{1,0:T(8,128)(2,1)S(1)}, bf16[256,256]{1,0:T(8,128)(2,1)S(1)}, u32[]{:S(2)}, u32[]{:S(2)}) collective-permute-start(bf16[256,256]{1,0:T(8,128)(2,1)S(1)} %collective-permute-done.8), channel_id=1, source_target_pairs={{0,1},{1,2},{2,3},{3,4},{4,5},{5,6},{6,7},{7,8},{8,9},{9,10},{10,1... | collective-permute-start | bytes 393224 | tf_op jit(solution)/shard_map/ppermute | solution.py:28
  105.5 5.6 %collective-permute-start.11 = (bf16[256,256]{1,0:T(8,128)(2,1)S(1)}, bf16[256,256]{1,0:T(8,128)(2,1)S(1)}, u32[]{:S(2)}, u32[]{:S(2)}) collective-permute-start(bf16[256,256]{1,0:T(8,128)(2,1)S(1)} %collective-permute-done.9), channel_id=1, source_target_pairs={{0,15},{1,0},{2,1},{3,2},{4,3},{5,4},{6,5},{7,6},{8,7},{9,8},{10,9... | collective-permute-start | bytes 393224 | tf_op jit(solution)/shard_map/ppermute | solution.py:33
  110.9 5.6 %collective-permute-start.12 = (bf16[256,256]{1,0:T(8,128)(2,1)S(1)}, bf16[256,256]{1,0:T(8,128)(2,1)S(1)}, u32[]{:S(2)}, u32[]{:S(2)}) collective-permute-start(bf16[256,256]{1,0:T(8,128)(2,1)S(1)} %collective-permute-done.10), channel_id=1, source_target_pairs={{0,1},{1,2},{2,3},{3,4},{4,5},{5,6},{6,7},{7,8},{8,9},{9,10},{10,1... | collective-permute-start | bytes 393224 | tf_op jit(solution)/shard_map/ppermute | solution.py:28
  111.0 5.6 %collective-permute-start.13 = (bf16[256,256]{1,0:T(8,128)(2,1)S(1)}, bf16[256,256]{1,0:T(8,128)(2,1)S(1)}, u32[]{:S(2)}, u32[]{:S(2)}) collective-permute-start(bf16[256,256]{1,0:T(8,128)(2,1)S(1)} %collective-permute-done.11), channel_id=1, source_target_pairs={{0,15},{1,0},{2,1},{3,2},{4,3},{5,4},{6,5},{7,6},{8,7},{9,8},{10,9... | collective-permute-start | bytes 393224 | tf_op jit(solution)/shard_map/ppermute | solution.py:33
  116.5 5.6 %collective-permute-start.14 = (bf16[256,256]{1,0:T(8,128)(2,1)S(1)}, bf16[256,256]{1,0:T(8,128)(2,1)S(1)}, u32[]{:S(2)}, u32[]{:S(2)}) collective-permute-start(bf16[256,256]{1,0:T(8,128)(2,1)S(1)} %collective-permute-done.12), channel_id=1, source_target_pairs={{0,1},{1,2},{2,3},{3,4},{4,5},{5,6},{6,7},{7,8},{8,9},{9,10},{10,1... | collective-permute-start | bytes 393224 | tf_op jit(solution)/shard_map/ppermute | solution.py:28
  122.8 0.6 copy-start.4
  123.5 13.1 %copy-start.15 = (s32[256,4]{0,1:T(4,128)S(1)}, s32[256,4]{0,1:T(4,128)}, u32[]{:S(2)}) copy-start(s32[256,4]{0,1:T(4,128)} %param.28) | copy-start | bytes 12292
  123.5 13.6 %copy-start.17 = (bf16[2048]{0:T(1024)(128)(2,1)S(1)}, bf16[2048]{0:T(1024)(128)(2,1)}, u32[]{:S(2)}) copy-start(bf16[2048]{0:T(1024)(128)(2,1)} %param.27) | copy-start | bytes 12292
  124.7 39.9 %all-to-all-start = ((bf16[16,256,128]{2,1,0:T(8,128)(2,1)}), bf16[16,256,128]{2,1,0:T(8,128)(2,1)S(1)}, u32[]{:S(2)}, u32[]{:S(2)}) async-start(bf16[16,256,128]{2,1,0:T(8,128)(2,1)} %broadcast_in_dim.91), calls=%async_computation | async-start | bytes 2097152 | tf_op jit(solution)/shard_map/all_to_all | solution.py:75
  195.8 3.8 %collective-permute-start.15 = (bf16[32,12,512]{2,1,0:T(8,128)(2,1)S(1)}, bf16[32,12,512]{2,1,0:T(8,128)(2,1)S(1)}, u32[]{:S(2)}, u32[]{:S(2)}) collective-permute-start(bf16[32,12,512]{2,1,0:T(8,128)(2,1)S(1)} %all_to_all.15), channel_id=1, source_target_pairs={{0,1},{1,0},{2,3},{3,2},{4,5},{5,4},{6,7},{7,6},{8,9},{9,8},{10,11... | collective-permute-start | bytes 1179656 | tf_op jit(solution)/shard_map/ppermute | solution.py:85
  201.3 21.2 %collective-permute-start.16 = (bf16[32,12,1024]{2,0,1:T(8,128)(2,1)}, bf16[32,12,1024]{2,0,1:T(8,128)(2,1)}, u32[]{:S(2)}, u32[]{:S(2)}) collective-permute-start(bf16[32,12,1024]{2,0,1:T(8,128)(2,1)} %copy.52), channel_id=1, source_target_pairs={{0,2},{1,3},{2,0},{3,1},{4,6},{5,7},{6,4},{7,5},{8,10},{9,11},{10,... | collective-permute-start | bytes 2359304 | tf_op jit(solution)/shard_map/ppermute | solution.py:85
  225.1 2.8 copy-start.3
  240.9 20.1 %collective-permute-start.17 = (bf16[384,4,2,128]{3,1,0,2:T(4,128)(2,1)S(1)}, bf16[384,4,2,128]{3,1,0,2:T(4,128)(2,1)}, u32[]{:S(2)}, u32[]{:S(2)}) collective-permute-start(bf16[384,4,2,128]{3,1,0,2:T(4,128)(2,1)S(1)} %bitcast.308), channel_id=1, source_target_pairs={{0,2},{1,3},{2,0},{3,1},{4,6},{5,7},{6,4},{7,5},{8,10},{9,11},{10,... | collective-permute-start | bytes 2359304 | tf_op jit(solution)/shard_map/ppermute | solution.py:85
  262.7 1.2 copy-start.1
  263.9 11.7 %copy-start.16 = (f32[256,4]{0,1:T(4,128)S(1)}, f32[256,4]{0,1:T(4,128)}, u32[]{:S(2)}) copy-start(f32[256,4]{0,1:T(4,128)} %param.29) | copy-start | bytes 12292
  263.9 12.5 %copy-start.8 = (bf16[2048,32]{0,1:T(8,128)(2,1)S(1)}, bf16[2048,32]{0,1:T(8,128)(2,1)}, u32[]{:S(2)}) copy-start(bf16[2048,32]{0,1:T(8,128)(2,1)} %param.33) | copy-start | bytes 393220
  264.0 5.1 %collective-permute-start.18 = (bf16[384,4,1,128]{3,1,0,2:T(4,128)(2,1)S(1)}, bf16[384,4,1,128]{3,1,0,2:T(4,128)(2,1)S(1)}, u32[]{:S(2)}, u32[]{:S(2)}) collective-permute-start(bf16[384,4,1,128]{3,1,0,2:T(4,128)(2,1)S(1)} %dynamic-slice_convert_fusion), channel_id=1, source_target_pairs={{0,1},{1,0},{2,3},{3,2},{4,5},{5,4},{6,7},{7,6},{8,9},{9,8},{10,11... | collective-permute-start | bytes 1179656 | tf_op jit(solution)/shard_map/ppermute | solution.py:85
  271.2 18.2 %all-to-all-start.2 = ((bf16[32,12,4,128]{3,2,1,0:T(4,128)(2,1)}), bf16[32,12,4,128]{3,2,1,0:T(4,128)(2,1)S(1)}, u32[]{:S(2)}, u32[]{:S(2)}) async-start(bf16[32,12,4,128]{3,2,1,0:T(4,128)(2,1)} %bitcast.64), calls=%async_computation.2 | async-start | bytes 786432 | tf_op jit(solution)/shard_map/all_to_all | solution.py:262
  293.0 7.0 %copy-start.9 = (bf16[2048,32]{0,1:T(8,128)(2,1)S(1)}, bf16[2048,32]{0,1:T(8,128)(2,1)}, u32[]{:S(2)}) copy-start(bf16[2048,32]{0,1:T(8,128)(2,1)} %param.34) | copy-start | bytes 393220
  293.0 7.0 %copy-start.10 = (f32[256,32]{0,1:T(8,128)S(1)}, f32[256,32]{0,1:T(8,128)}, u32[]{:S(2)}) copy-start(f32[256,32]{0,1:T(8,128)} %fusion.143) | copy-start | bytes 98308
  295.8 26.6 %copy-start.12 = (bf16[512,128]{1,0:T(8,128)(2,1)S(1)}, bf16[512,128]{1,0:T(8,128)(2,1)}, u32[]{:S(2)}) copy-start(bf16[512,128]{1,0:T(8,128)(2,1)} %param.35) | copy-start | bytes 393220
  295.8 32.8 %copy-start.5 = (bf16[256,128]{1,0:T(8,128)(2,1)S(1)}, bf16[256,128]{1,0:T(8,128)(2,1)}, u32[]{:S(2)}) copy-start(bf16[256,128]{1,0:T(8,128)(2,1)} %copy-done.4) | copy-start | bytes 196612
  295.9 24.5 %collective-permute-start.19 = (bf16[256,2,128]{2,0,1:T(8,128)(2,1)S(1)}, bf16[256,2,128]{2,0,1:T(8,128)(2,1)S(1)}, u32[]{:S(2)}, u32[]{:S(2)}) collective-permute-start(bf16[256,2,128]{2,0,1:T(8,128)(2,1)S(1)} %fusion.50), channel_id=1, source_target_pairs={{0,8},{1,9},{2,10},{3,11},{4,12},{5,13},{6,14},{7,15},{8,0},{9,1},... | collective-permute-start | bytes 393224 | tf_op jit(solution)/shard_map/ppermute | solution.py:85
  320.4 8.2 %collective-permute-start.20 = (bf16[256,1,128]{2,0,1:T(8,128)(2,1)S(1)}, bf16[256,1,128]{2,0,1:T(8,128)(2,1)S(1)}, u32[]{:S(2)}, u32[]{:S(2)}) collective-permute-start(bf16[256,1,128]{2,0,1:T(8,128)(2,1)S(1)} %dynamic-slice_convert_fusion.2), channel_id=1, source_target_pairs={{0,4},{1,5},{2,6},{3,7},{4,0},{5,1},{6,2},{7,3},{8,12},{9,13},{10,... | collective-permute-start | bytes 196616 | tf_op jit(solution)/shard_map/ppermute | solution.py:85
